TPU v7x, 128 devices: a whole 4x4x4 slice. The times are simulated.
128 devices in a mesh: sp: 16 (over z, y), dp: 8 (over x, core).
Axes of the slice: x: 4, y: 4, z: 4, core: 2. Of those that a mesh axis runs over, the one named last changes fastest.
Arguments:
- u_pre: bfloat16 [8, 16384, 2048], P('dp', 'sp'), may hold values from -6 to 6
- v_pre: bfloat16 [8, 16384, 2048], P('dp', 'sp'), may hold values from -6 to 6
- d_out: bfloat16 [8, 16384, 2048], P('dp', 'sp'), may hold values from -6 to 6
- w_mix: bfloat16 [16, 128, 128], replicated, may hold values from -0.5 to 0.5
- mix_bias: float32 [16, 128], replicated, may hold values from 0.1 to 1.9
- norm_gain: float32 [16, 128], replicated, may hold values from 0.1 to 1.9
- norm_shift: float32 [16, 128], replicated, may hold values from -3 to 3
- w_out: bfloat16 [2048, 2048], P('dp'), may hold values from -0.125 to 0.125
Outputs:
- grad_u: bfloat16 [8, 16384, 2048], P('dp', 'sp')
- grad_v: bfloat16 [8, 16384, 2048], P('dp', 'sp')
- grad_w_out: float32 [2048, 2048], P('dp')
- grad_w_mix: float32 [16, 128, 128], replicated
- grad_mix_bias: float32 [16, 128], replicated
- grad_gain: float32 [16, 128], replicated
- grad_shift: float32 [16, 128], replicated
All inputs are finite; a program needn't handle non-finite values.
Results may differ from a plain program's by a relative error of at most 0.012.
Values may be sent and summed in bfloat16 or wider, within the bound.
A program may use at most 192 MiB of HBM per device.

v0:
```python
import jax
import jax.numpy as jnp
from jax import lax
from jax.sharding import PartitionSpec as P

EPS = 1e-05


def together(arrays, axis):
    ends = [0]
    for a in arrays:
        ends.append(ends[-1] + a.size)
    total = lax.psum(jnp.concatenate([a.ravel() for a in arrays]), axis)
    return tuple((total[b:e].reshape(a.shape) for a, b, e in zip(arrays, ends, ends[1:])))


def mechanism(grad_s, u_pre, v_pre, w_mix, mix_bias, gain, shift):
    items, length, width = grad_s.shape
    groups, span = (w_mix.shape[0], w_mix.shape[1])
    chans = width // groups
    shape = (items, length // span, span, groups, chans)
    u_val = u_pre.astype(jnp.float32).reshape(shape)
    v_val = v_pre.astype(jnp.float32).reshape(shape)
    cotan = grad_s.astype(jnp.float32).reshape(shape)
    upper, u_back = jax.vjp(jax.nn.gelu, u_val)
    gated, v_back = jax.vjp(jax.nn.gelu, v_val)
    centre = gated - jnp.mean(gated, axis=-1, keepdims=True)
    inverse = lax.rsqrt(jnp.mean(centre * centre, axis=-1, keepdims=True) + EPS)
    scaled = centre * inverse
    normed = (scaled * gain + shift).astype(jnp.bfloat16)
    lower = jnp.tril(jnp.ones((span, span), dtype=bool))
    w_low = jnp.where(lower[None], w_mix, jnp.zeros_like(w_mix))
    mixed = jnp.einsum("gts,insgc->intgc", w_low, normed, preferred_element_type=jnp.float32)
    mixed = mixed + jnp.transpose(mix_bias)[:, :, None]
    gated_out = (upper * mixed).astype(jnp.bfloat16)
    d_mixed = cotan * upper
    d_mixed_b = d_mixed.astype(jnp.bfloat16)
    grad_u = u_back(cotan * mixed)[0].astype(jnp.bfloat16).reshape(items, length, width)
    grad_bias = jnp.transpose(jnp.sum(d_mixed, axis=(0, 1, 4)))
    grad_w = jnp.einsum("intgc,insgc->gts", d_mixed_b, normed, preferred_element_type=jnp.float32)
    grad_w = jnp.where(lower[None], grad_w, jnp.zeros_like(grad_w))
    d_normed = jnp.einsum("gts,intgc->insgc", w_low, d_mixed_b, preferred_element_type=jnp.float32)
    grad_gain = jnp.sum(d_normed * scaled, axis=(0, 1, 2))
    grad_shift = jnp.sum(d_normed, axis=(0, 1, 2))
    d_scaled = d_normed * gain
    d_gated = inverse * (
        d_scaled
        - jnp.mean(d_scaled, axis=-1, keepdims=True)
        - scaled * jnp.mean(d_scaled * scaled, axis=-1, keepdims=True)
    )
    grad_v = v_back(d_gated)[0].astype(jnp.bfloat16).reshape(items, length, width)
    return (
        grad_u,
        grad_v,
        gated_out.reshape(items, length, width),
        grad_w,
        grad_bias,
        grad_gain,
        grad_shift,
    )


def on_device(u_pre, v_pre, d_out, w_mix, mix_bias, norm_gain, norm_shift, w_out):
    grad_s = lax.dot_general(
        d_out,
        lax.all_gather(w_out, "dp", axis=0, tiled=True),
        (((2,), (1,)), ((), ())),
        preferred_element_type=jnp.float32,
    ).astype(jnp.bfloat16)
    grad_u, grad_v, gated_out, grad_w, grad_bias, grad_gain, grad_shift = mechanism(
        grad_s, u_pre, v_pre, w_mix, mix_bias, norm_gain, norm_shift
    )
    grad_w, grad_bias, grad_gain, grad_shift = together(
        (grad_w, grad_bias, grad_gain, grad_shift), ("sp", "dp")
    )
    width = gated_out.shape[2]
    flat_d = d_out.reshape(-1, d_out.shape[2])
    flat_s = gated_out.reshape(-1, width)
    partial_rows = lax.psum_scatter(
        lax.dot_general(
            flat_s, flat_d, (((0,), (0,)), ((), ())), preferred_element_type=jnp.float32
        ),
        "dp",
        scatter_dimension=0,
        tiled=True,
    )
    grad_w_out = lax.psum(partial_rows, "sp")
    return (grad_u, grad_v, grad_w_out, grad_w, grad_bias, grad_gain, grad_shift)


def solution(mesh):
    return jax.shard_map(
        on_device,
        mesh=mesh,
        in_specs=(
            P("dp", "sp", None),
            P("dp", "sp", None),
            P("dp", "sp", None),
            P(),
            P(),
            P(),
            P(),
            P("dp", None),
        ),
        out_specs=(P("dp", "sp", None), P("dp", "sp", None), P("dp", None), P(), P(), P(), P()),
        check_vma=False,
    )
```

profile of v0, /device:TPU:0, one launch (start us, length us, event | category | flops | bytes accessed | tf_op | source)
XLA Modules:
  0.0 474.1 jit_solution(16673040196392679940)
XLA Ops:
  7.2 0.0 all-gather.2.cloned.1.call-start
  7.2 0.7 all-gather.2.cloned.1.call-update
  7.9 0.0 reduce-scatter.2.cloned.1.call-start
  7.9 3.2 convert_bitcast_fusion
  11.2 5.2 %copy.67 = f32[128,8,16,128]{3,2,1,0:T(8,128)} copy(f32[128,8,16,128]{3,1,2,0:T(8,128)S(1)} %convert_bitcast_fusion) | data formatting | bytes 16777216
  16.4 9.1 %copy.45 = f32[1,8,128,16,128]{2,4,1,3,0:T(8,128)} copy(f32[1,8,128,16,128]{4,3,0,2,1:T(8,128)} %bitcast.100) | data formatting | bytes 16777216 | tf_op jit(solution)/shard_map/reshape | solution.py:22
  25.5 3.2 convert_bitcast_fusion.1
  28.8 5.2 %copy.65 = f32[128,8,16,128]{3,2,1,0:T(8,128)} copy(f32[128,8,16,128]{3,1,2,0:T(8,128)S(1)} %convert_bitcast_fusion.1) | data formatting | bytes 16777216
  34.0 8.7 %copy.39 = f32[1,8,128,16,128]{2,4,1,3,0:T(8,128)} copy(f32[1,8,128,16,128]{4,3,0,2,1:T(8,128)} %bitcast.104) | data formatting | bytes 16777216 | tf_op jit(solution)/shard_map/reshape | solution.py:23
  42.7 0.0 copy-start
  42.7 0.0 copy-start.1
  42.7 0.0 copy-start.3
  42.7 0.0 copy-start.4
  42.8 5.9 %fusion.54 = f32[8,128,16]{1,0,2:T(8,128)S(1)} fusion(f32[1,8,128,16,128]{2,4,1,3,0:T(8,128)} %copy.39), kind=kLoop, calls=%fused_computation.83 | loop fusion | flops 18857984 | bytes 8454144 | tf_op jit(solution)/shard_map/reduce_sum | solution.py:27
  48.6 0.2 copy-done
  48.9 3.7 multiply_reduce_fusion.2
  52.6 0.0 copy-done.1
  52.6 0.0 copy-done.3
  52.7 0.0 copy-done.4
  52.7 6.5 %fusion.35 = bf16[8,128,16,128]{3,1,0,2:T(8,128)(2,1)} fusion(f32[8,128,16,128]{3,2,1,0:T(8,128)S(1)} %bitcast.105, f32[16,128]{1,0:T(8,128)S(1)} %copy-done.4, f32[16,128]{1,0:T(8,128)S(1)} %copy-done.3, f32[8,128,16]{1,0,2:T(8,128)S(1)} %add_rsqrt_fusion, f32[8,128,16]{1,0,2:T(8,128)S(1)} %broadcast_multiply_fusion.2), kind=kLoop, calls=%fused_computation.52 | loop fusion | flops 27262976 | bytes 12730368 | tf_op jit(solution)/shard_map/convert_element_type | solution.py:30
  59.1 2.7 all-gather.2.cloned.1.call-done
  61.8 13.1 %convert_bitcast_fusion.2 = f32[128,8,16,128]{3,1,2,0:T(8,128)S(1)} fusion(bf16[2048,2048]{1,0:T(8,128)(2,1)} %all-gather.2.cloned.1.call-done, bf16[1,1024,2048]{2,1,0:T(8,128)(2,1)} %param.10), kind=kOutput, calls=%fused_computation.51 | convolution fusion | flops 8594128896 | bytes 20971520 | tf_op jit(solution)/shard_map/dot_general | solution.py:64
  74.9 5.2 %copy.64 = f32[128,8,16,128]{3,2,1,0:T(8,128)} copy(f32[128,8,16,128]{3,1,2,0:T(8,128)S(1)} %convert_bitcast_fusion.2) | data formatting | bytes 16777216
  80.1 0.0 copy-start.5
  80.1 0.0 copy-start.6
  80.1 8.8 %copy.41 = f32[1,8,128,16,128]{2,4,1,3,0:T(8,128)} copy(f32[1,8,128,16,128]{4,3,2,1,0:T(8,128)} %bitcast.102) | data formatting | bytes 16777216 | tf_op jit(solution)/shard_map/reshape | solution.py:24
  88.9 0.0 copy-done.5
  88.9 0.0 copy-done.6
  88.9 14.8 %multiply_convert_fusion = (bf16[1,8,128,16,128]{2,4,1,3,0:T(8,128)(2,1)}, bf16[1,8,128,16,128]{2,4,1,3,0:T(8,128)(2,1)}, f32[128,16]{0,1:T(8,128)S(1)}) fusion(f32[128,16]{0,1:T(8,128)S(1)} %bitcast.112, f32[1,8,128,16,128]{2,4,1,3,0:T(8,128)} %copy.45, f32[1,8,128,16,128]{2,4,1,3,0:T(8,128)} %copy.41, bf16[8,128,16,128]{3,1,0,2:T(8,128)(2,1)} %fusion.35, ...), kind=kOutput, calls=%fused_computation.46 | convolution fusion | flops 593754112 | bytes 29917184 | tf_op jit(solution)/shard_map/gts,insgc->intgc/dot_general | solution.py:33
  103.7 6.8 %copy.58 = bf16[1,8,128,16,128]{4,3,2,1,0:T(8,128)(2,1)} copy(bf16[1,8,128,16,128]{2,4,1,3,0:T(8,128)(2,1)} %get-tuple-element.11) | data formatting | bytes 8388608 | tf_op jit(solution)/shard_map/convert_element_type | solution.py:35
  110.5 15.4 %fusion.37 = f32[2048,2048]{1,0:T(8,128)} fusion(bf16[128,8,16,128]{3,2,1,0:T(8,128)(2,1)} %bitcast.107, bf16[1,1024,2048]{2,1,0:T(8,128)(2,1)} %param.10), kind=kOutput, calls=%fused_computation.57 | convolution fusion | flops 8589934592 | bytes 25165824 | tf_op jit(solution)/shard_map/dot_general | solution.py:80
  125.9 0.0 reduce-scatter.2.cloned.1.call-update
  125.9 0.0 all-reduce.5.cloned.1.call-start
  125.9 0.0 copy-start.2
  125.9 10.2 %fusion.33 = bf16[8,128,16,128]{3,1,0,2:T(8,128)(2,1)S(1)} fusion(f32[8,128,16,128]{3,2,1,0:T(8,128)} %bitcast.103, f32[8,128,16,128]{3,2,1,0:T(8,128)} %bitcast.101), kind=kLoop, calls=%fused_computation.39 | loop fusion | flops 20971520 | bytes 20971520 | tf_op jit(solution)/shard_map/convert_element_type | solution.py:37
  136.1 0.0 copy-done.2
  136.2 1.3 fusion.45
  137.4 10.3 %fusion.34 = (f32[16,128]{1,0:T(8,128)S(1)}, f32[8,128,16]{1,0,2:T(8,128)S(1)}, f32[8,128,16]{1,0,2:T(8,128)S(1)}, f32[16,128]{1,0:T(8,128)S(1)}, f32[16,8,128,128]{3,2,1,0:T(8,128)}) fusion(f32[8,128,16]{1,0,2:T(8,128)S(1)} %add_rsqrt_fusion, f32[8,128,16]{1,0,2:T(8,128)S(1)} %broadcast_multiply_fusion.2, f32[1,8,128,16,128]{2,4,1,3,0:T(8,128)} %copy.39, ...), kind=kOutput, calls=%fused_computation.44 | convolution fusion | flops 572747776 | bytes 21798912 | tf_op jit(solution)/shard_map/gts,intgc->insgc/dot_general | solution.py:42
  147.7 1.0 pad_maximum_fusion
  148.8 0.0 all-reduce.5.cloned.1.call-update
  148.8 0.0 all-reduce.3.cloned.1.call-start
  148.9 7.0 %copy.47 = bf16[1,8,128,16,128]{4,3,2,1,0:T(8,128)(2,1)} copy(bf16[1,8,128,16,128]{2,4,1,3,0:T(8,128)(2,1)} %get-tuple-element.12) | data formatting | bytes 8388608 | tf_op jit(solution)/shard_map/convert_element_type | solution.py:38
  155.8 7.3 %reshape.497 = bf16[1,1024,2048]{2,1,0:T(8,128)(2,1)} reshape(bf16[1,8,128,16,128]{4,3,2,1,0:T(8,128)(2,1)} %copy.47) | data formatting | bytes 8388608 | tf_op jit(solution)/shard_map/reshape | solution.py:38
  163.2 54.8 %reduce-scatter.2.cloned.1.call-done = f32[256,2048]{1,0:T(8,128)} async-done(((f32[2048,2048]{1,0:T(8,128)}), f32[256,2048]{1,0:T(8,128)}) %reduce-scatter.2.cloned.1.call-update) | async-done | bytes 2097168 | tf_op jit(solution)/shard_map/reduce_scatter | solution.py:79
  217.9 0.0 all-reduce.3.cloned.1.call-update
  218.0 12.0 %fusion.6 = bf16[1,8,128,16,128]{2,4,1,3,0:T(8,128)(2,1)} fusion(f32[1,8,128,16,128]{2,4,1,3,0:T(8,128)} %copy.39, f32[16,8,128,128]{3,2,1,0:T(8,128)} %get-tuple-element.17, f32[8,128,16]{1,0,2:T(8,128)S(1)} %get-tuple-element.18, f32[8,128,16]{1,0,2:T(8,128)S(1)} %get-tuple-element.19, f32[16,128]{1,0:T(8,128)S(1)} %copy-done.3, ...), kind=kLoop, calls=%fused_computation.12 | loop fusion | flops 58720256 | bytes 21241856 | tf_op jit(solution)/shard_map/convert_element_type | solution.py:51
  230.0 6.7 %copy.56 = bf16[1,8,128,16,128]{4,3,2,1,0:T(8,128)(2,1)} copy(bf16[1,8,128,16,128]{2,4,1,3,0:T(8,128)(2,1)} %fusion.6) | data formatting | bytes 8388608 | tf_op jit(solution)/shard_map/convert_element_type | solution.py:51
  236.8 7.3 %reshape.500 = bf16[1,1024,2048]{2,1,0:T(8,128)(2,1)} reshape(bf16[1,8,128,16,128]{4,3,2,1,0:T(8,128)(2,1)} %copy.56) | data formatting | bytes 8388608 | tf_op jit(solution)/shard_map/reshape | solution.py:51
  244.1 127.2 %all-reduce.5.cloned.1.call-done = f32[268288]{0:T(1024)} async-done(((f32[268288]{0:T(1024)}), f32[268288]{0:T(1024)}) %all-reduce.5.cloned.1.call-update) | async-done | bytes 1073168 | tf_op jit(solution)/shard_map/psum | solution.py:13
  371.2 2.3 slice.49
  373.5 1.3 slice_bitcast_fusion
  374.8 89.4 %all-reduce.3.cloned.1.call-done = f32[256,2048]{1,0:T(8,128)} async-done(((f32[256,2048]{1,0:T(8,128)}), f32[256,2048]{1,0:T(8,128)}) %all-reduce.3.cloned.1.call-update) | async-done | bytes 2097168 | tf_op jit(solution)/shard_map/psum | solution.py:87
  464.2 3.1 copy.82
  (4 shorter events, 0.1 us)
Async XLA Ops:
  7.2 54.7 %all-gather.2.cloned.1.call-start = ((), (), s32[]{:S(2)}) async-start(), calls=%async_computation.1 | async-start | bytes 9437184 | tf_op jit(solution)/shard_map/all_gather | solution.py:66
  7.9 210.1 %reduce-scatter.2.cloned.1.call-start = ((), (), s32[]{:S(2)}) async-start(), calls=%async_computation.2 | async-start | bytes 18874368 | tf_op jit(solution)/shard_map/reduce_scatter | solution.py:79
  42.7 6.2 %copy-start = (f32[1,8,128,16,128]{2,4,1,3,0:T(8,128)S(1)}, f32[1,8,128,16,128]{2,4,1,3,0:T(8,128)}, u32[]{:S(2)}) copy-start(f32[1,8,128,16,128]{2,4,1,3,0:T(8,128)} %copy.39) | copy-start | bytes 25165828
  42.7 9.9 %copy-start.1 = (f32[128,8,16,128]{3,2,1,0:T(8,128)S(1)}, f32[128,8,16,128]{3,2,1,0:T(8,128)}, u32[]{:S(2)}) copy-start(f32[128,8,16,128]{3,2,1,0:T(8,128)} %copy.65) | copy-start | bytes 25165828
  42.7 9.9 %copy-start.3 = (f32[16,128]{1,0:T(8,128)S(1)}, f32[16,128]{1,0:T(8,128)}, u32[]{:S(2)}) copy-start(f32[16,128]{1,0:T(8,128)} %param.13) | copy-start | bytes 24580
  42.7 9.9 %copy-start.4 = (f32[16,128]{1,0:T(8,128)S(1)}, f32[16,128]{1,0:T(8,128)}, u32[]{:S(2)}) copy-start(f32[16,128]{1,0:T(8,128)} %param.14) | copy-start | bytes 24580
  80.1 8.8 %copy-start.5 = (bf16[16,128,128]{2,1,0:T(8,128)(2,1)S(1)}, bf16[16,128,128]{2,1,0:T(8,128)(2,1)}, u32[]{:S(2)}) copy-start(bf16[16,128,128]{2,1,0:T(8,128)(2,1)} %param.11) | copy-start | bytes 1572868
  80.1 8.8 %copy-start.6 = (f32[16,128]{1,0:T(8,128)S(1)}, f32[16,128]{1,0:T(8,128)}, u32[]{:S(2)}) copy-start(f32[16,128]{1,0:T(8,128)} %param.12) | copy-start | bytes 24580
  125.9 245.4 %all-reduce.5.cloned.1.call-start = ((), (), s32[]{:S(2)}) async-start(), calls=%async_computation.4 | async-start | bytes 2146304 | tf_op jit(solution)/shard_map/psum | solution.py:13
  125.9 10.2 %copy-start.2 = (bf16[8,128,16,128]{3,1,0,2:T(8,128)(2,1)S(1)}, bf16[8,128,16,128]{3,1,0,2:T(8,128)(2,1)}, u32[]{:S(2)}) copy-start(bf16[8,128,16,128]{3,1,0,2:T(8,128)(2,1)} %fusion.35) | copy-start | bytes 12582916
  148.8 315.4 %all-reduce.3.cloned.1.call-start = ((), (), s32[]{:S(2)}) async-start(), calls=%async_computation.3 | async-start | bytes 4194304 | tf_op jit(solution)/shard_map/psum | solution.py:87
Sparse Core Ops, SparseCore 0:
  9.7 52.0 all-gather.1
  126.0 91.9 reduce-scatter.1
  223.3 147.8 all-reduce.4
  374.4 89.7 all-reduce.2
where the time goes:
time: 478 us; the launch traced here: 474 us
  waiting for transfers between devices  275 us (58%)
  local copies, waits for them, and re-layouts  84.4 us (18%)
  matrix products  54.8 us (11%)
  other arithmetic  45.8 us (10%)
  between operations  14.1 us (3%)
    psum x1, waiting for transfers between devices, together(): total = lax.psum(jnp.concatenate([a.ravel() for a in arrays]), axis)  127 us
    psum x1, waiting for transfers between devices, on_device(): grad_w_out = lax.psum(partial_rows, 'sp')  89.4 us
    reduce_scatter x1, waiting for transfers between devices, on_device(): lax.psum_scatter(lax.dot_general(flat_s, flat_d, (((0,), (0,)), ((), ()))...  54.8 us
    unnamed x18, local copies, waits for them, and re-layouts  19 us
    dot_general x1, matrix products, on_device(): lax.dot_general(flat_s, flat_d, (((0,), (0,)), ((), ())), preferred_eleme...  15.4 us
    dot_general x1, matrix products, mechanism(): jnp.einsum('gts,insgc->intgc', w_low, normed, preferred_element_type=jnp....  14.8 us
    dot_general x1, matrix products, on_device(): lax.dot_general(d_out, lax.all_gather(w_out, 'dp', axis=0, tiled=True), (...  13.1 us
    convert_element_type x1, other arithmetic, mechanism(): v_back(d_gated)[0].astype(jnp.bfloat16).reshape(items, length, width)  12 us
  transfers between devices with their start and end apart: 4, of which 4 were waited for; matrix products, arithmetic and copies ran while one was open for 25% of the time, Pallas kernels for 0%

commit v1 on v0

--- a/solution.py
+++ b/solution.py
@@ -1,9 +1,18 @@
+import functools
 import jax
 import jax.numpy as jnp
 from jax import lax
 from jax.sharding import PartitionSpec as P
 
 EPS = 1e-05
+
+
+def use_leaf(w_in, comm_axis):
+    val = lax.all_gather(w_in, comm_axis)
+    return jnp.sum(val, 0)
+
+
+order_patches = functools.partial(use_leaf, comm_axis="sp")
 
 
 def together(arrays, axis):
@@ -84,7 +93,7 @@
         scatter_dimension=0,
         tiled=True,
     )
-    grad_w_out = lax.psum(partial_rows, "sp")
+    grad_w_out = order_patches(partial_rows)
     return (grad_u, grad_v, grad_w_out, grad_w, grad_bias, grad_gain, grad_shift)
 
 

time: 478 us -> 594 us (1.24)
  waiting for transfers between devices: 275 us -> 379 us
  other arithmetic: 45.8 us -> 59.3 us
    all_gather x0 -> x1, waiting for transfers between devices: none -> 194 us  [use_leaf(): val = lax.all_gather(w_in, comm_axis)]
    psum x1 -> x0, waiting for transfers between devices: 89.4 us -> none  [on_device(): grad_w_out = lax.psum(partial_rows, 'sp')]
    psum x1, waiting for transfers between devices: 127 us -> 113 us  [together(): total = lax.psum(jnp.concatenate([a.ravel() for a in arrays]), axis)]
    reduce_scatter x1, waiting for transfers between devices: 54.8 us -> 69.1 us  [on_device(): lax.psum_scatter(lax.dot_general(flat_s, flat_d, (((0,), (0,)), ((), ()))...]
    reduce_sum x0 -> x1, other arithmetic: none -> 13.1 us  [use_leaf(): return jnp.sum(val, 0)]
    unnamed x18 -> x17, local copies, waits for them, and re-layouts: 19 us -> 15.7 us
  transfers between devices with their start and end apart: 4 -> 4, of which waited for: 4 -> 4; matrix products, arithmetic and copies ran while one was open for 25% -> 20% of each run, Pallas kernels for 0% -> 0%
where the time goes in v1:
time: 594 us; the launch traced here: 589 us
  waiting for transfers between devices  379 us (64%)
  local copies, waits for them, and re-layouts  81 us (14%)
  other arithmetic  59.3 us (10%)
  matrix products  54.9 us (9%)
  between operations  14.1 us (2%)
    all_gather x1, waiting for transfers between devices, use_leaf(): val = lax.all_gather(w_in, comm_axis)  194 us
    psum x1, waiting for transfers between devices, together(): total = lax.psum(jnp.concatenate([a.ravel() for a in arrays]), axis)  113 us
    reduce_scatter x1, waiting for transfers between devices, on_device(): lax.psum_scatter(lax.dot_general(flat_s, flat_d, (((0,), (0,)), ((), ()))...  69.1 us
    unnamed x17, local copies, waits for them, and re-layouts  15.7 us
    dot_general x1, matrix products, on_device(): lax.dot_general(flat_s, flat_d, (((0,), (0,)), ((), ())), preferred_eleme...  15.4 us
    dot_general x1, matrix products, mechanism(): jnp.einsum('gts,insgc->intgc', w_low, normed, preferred_element_type=jnp....  14.9 us
    reduce_sum x1, other arithmetic, use_leaf(): return jnp.sum(val, 0)  13.1 us
    dot_general x1, matrix products, on_device(): lax.dot_general(d_out, lax.all_gather(w_out, 'dp', axis=0, tiled=True), (...  13.1 us
  transfers between devices with their start and end apart: 4, of which 4 were waited for; matrix products, arithmetic and copies ran while one was open for 20% of the time, Pallas kernels for 0%

profile of v1, /device:TPU:0, one launch (start us, length us, event | category | flops | bytes accessed | tf_op | source)
XLA Modules:
  0.0 589.0 jit_solution(8705468033260390832)
XLA Ops:
  7.2 0.0 all-gather.4.cloned.1.call-start
  7.2 0.7 all-gather.4.cloned.1.call-update
  7.9 0.0 reduce-scatter.2.cloned.1.call-start
  7.9 3.2 convert_bitcast_fusion
  11.2 5.2 copy.67
  16.4 9.1 %copy.45 = f32[1,8,128,16,128]{2,4,1,3,0:T(8,128)} copy(f32[1,8,128,16,128]{4,3,0,2,1:T(8,128)} %bitcast.101) | data formatting | bytes 16777216 | tf_op jit(solution)/shard_map/reshape | solution.py:31
  25.5 3.2 convert_bitcast_fusion.1
  28.8 5.2 copy.65
  34.0 8.7 %copy.39 = f32[1,8,128,16,128]{2,4,1,3,0:T(8,128)} copy(f32[1,8,128,16,128]{4,3,0,2,1:T(8,128)} %bitcast.105) | data formatting | bytes 16777216 | tf_op jit(solution)/shard_map/reshape | solution.py:32
  42.7 0.0 copy-start
  42.7 0.0 copy-start.1
  42.7 0.0 copy-start.3
  42.7 0.0 copy-start.4
  42.8 6.0 %fusion.54 = f32[8,128,16]{1,0,2:T(8,128)S(1)} fusion(f32[1,8,128,16,128]{2,4,1,3,0:T(8,128)} %copy.39), kind=kLoop, calls=%fused_computation.83 | loop fusion | flops 18857984 | bytes 8454144 | tf_op jit(solution)/shard_map/reduce_sum | solution.py:36
  48.8 0.1 copy-done
  48.9 3.7 multiply_reduce_fusion.2
  52.6 0.0 copy-done.1
  52.7 0.0 copy-done.3
  52.7 0.0 copy-done.4
  52.7 6.5 %fusion.35 = bf16[8,128,16,128]{3,1,0,2:T(8,128)(2,1)} fusion(f32[8,128,16,128]{3,2,1,0:T(8,128)S(1)} %bitcast.106, f32[16,128]{1,0:T(8,128)S(1)} %copy-done.4, f32[16,128]{1,0:T(8,128)S(1)} %copy-done.3, f32[8,128,16]{1,0,2:T(8,128)S(1)} %add_rsqrt_fusion, f32[8,128,16]{1,0,2:T(8,128)S(1)} %broadcast_multiply_fusion.2), kind=kLoop, calls=%fused_computation.52 | loop fusion | flops 27262976 | bytes 12730368 | tf_op jit(solution)/shard_map/convert_element_type | solution.py:39
  59.1 2.7 all-gather.4.cloned.1.call-done
  61.8 13.1 %convert_bitcast_fusion.2 = f32[128,8,16,128]{3,1,2,0:T(8,128)S(1)} fusion(bf16[2048,2048]{1,0:T(8,128)(2,1)} %all-gather.4.cloned.1.call-done, bf16[1,1024,2048]{2,1,0:T(8,128)(2,1)} %param.10), kind=kOutput, calls=%fused_computation.51 | convolution fusion | flops 8594128896 | bytes 20971520 | tf_op jit(solution)/shard_map/dot_general | solution.py:73
  74.9 5.2 copy.64
  80.1 0.0 copy-start.5
  80.1 0.0 copy-start.6
  80.1 8.8 %copy.41 = f32[1,8,128,16,128]{2,4,1,3,0:T(8,128)} copy(f32[1,8,128,16,128]{4,3,2,1,0:T(8,128)} %bitcast.103) | data formatting | bytes 16777216 | tf_op jit(solution)/shard_map/reshape | solution.py:33
  88.9 0.0 copy-done.5
  88.9 0.0 copy-done.6
  88.9 14.9 %multiply_convert_fusion = (bf16[1,8,128,16,128]{2,4,1,3,0:T(8,128)(2,1)}, bf16[1,8,128,16,128]{2,4,1,3,0:T(8,128)(2,1)}, f32[128,16]{0,1:T(8,128)S(1)}) fusion(f32[128,16]{0,1:T(8,128)S(1)} %bitcast.114, f32[1,8,128,16,128]{2,4,1,3,0:T(8,128)} %copy.45, f32[1,8,128,16,128]{2,4,1,3,0:T(8,128)} %copy.41, bf16[8,128,16,128]{3,1,0,2:T(8,128)(2,1)} %fusion.35, ...), kind=kOutput, calls=%fused_computation.46 | convolution fusion | flops 593754112 | bytes 29917184 | tf_op jit(solution)/shard_map/gts,insgc->intgc/dot_general | solution.py:42
  103.8 6.8 %copy.58 = bf16[1,8,128,16,128]{4,3,2,1,0:T(8,128)(2,1)} copy(bf16[1,8,128,16,128]{2,4,1,3,0:T(8,128)(2,1)} %get-tuple-element.11) | data formatting | bytes 8388608 | tf_op jit(solution)/shard_map/convert_element_type | solution.py:44
  110.6 15.4 %fusion.37 = f32[2048,2048]{1,0:T(8,128)} fusion(bf16[128,8,16,128]{3,2,1,0:T(8,128)(2,1)} %bitcast.109, bf16[1,1024,2048]{2,1,0:T(8,128)(2,1)} %param.10), kind=kOutput, calls=%fused_computation.57 | convolution fusion | flops 8589934592 | bytes 25165824 | tf_op jit(solution)/shard_map/dot_general | solution.py:89
  125.9 0.0 reduce-scatter.2.cloned.1.call-update
  126.0 0.0 all-reduce.2.cloned.1.call-start
  126.0 0.0 copy-start.2
  126.0 10.2 %fusion.33 = bf16[8,128,16,128]{3,1,0,2:T(8,128)(2,1)S(1)} fusion(f32[8,128,16,128]{3,2,1,0:T(8,128)} %bitcast.104, f32[8,128,16,128]{3,2,1,0:T(8,128)} %bitcast.102), kind=kLoop, calls=%fused_computation.39 | loop fusion | flops 20971520 | bytes 20971520 | tf_op jit(solution)/shard_map/convert_element_type | solution.py:46
  136.2 0.0 copy-done.2
  136.2 1.3 fusion.45
  137.5 10.3 %fusion.34 = (f32[16,128]{1,0:T(8,128)S(1)}, f32[8,128,16]{1,0,2:T(8,128)S(1)}, f32[8,128,16]{1,0,2:T(8,128)S(1)}, f32[16,128]{1,0:T(8,128)S(1)}, f32[16,8,128,128]{3,2,1,0:T(8,128)}) fusion(f32[8,128,16]{1,0,2:T(8,128)S(1)} %add_rsqrt_fusion, f32[8,128,16]{1,0,2:T(8,128)S(1)} %broadcast_multiply_fusion.2, f32[1,8,128,16,128]{2,4,1,3,0:T(8,128)} %copy.39, ...), kind=kOutput, calls=%fused_computation.44 | convolution fusion | flops 572747776 | bytes 21798912 | tf_op jit(solution)/shard_map/gts,intgc->insgc/dot_general | solution.py:51
  147.8 1.0 pad_maximum_fusion
  148.9 0.0 all-reduce.2.cloned.1.call-update
  148.9 0.0 all-gather.6.cloned.1.call-start
  148.9 69.1 %reduce-scatter.2.cloned.1.call-done = f32[256,2048]{1,0:T(8,128)} async-done(((f32[2048,2048]{1,0:T(8,128)}), f32[256,2048]{1,0:T(8,128)}) %reduce-scatter.2.cloned.1.call-update) | async-done | bytes 2097168 | tf_op jit(solution)/shard_map/reduce_scatter | solution.py:88
  218.1 0.0 all-gather.6.cloned.1.call-update
  218.1 6.9 %copy.47 = bf16[1,8,128,16,128]{4,3,2,1,0:T(8,128)(2,1)} copy(bf16[1,8,128,16,128]{2,4,1,3,0:T(8,128)(2,1)} %get-tuple-element.12) | data formatting | bytes 8388608 | tf_op jit(solution)/shard_map/convert_element_type | solution.py:47
  225.0 7.3 %reshape.497 = bf16[1,1024,2048]{2,1,0:T(8,128)(2,1)} reshape(bf16[1,8,128,16,128]{4,3,2,1,0:T(8,128)(2,1)} %copy.47) | data formatting | bytes 8388608 | tf_op jit(solution)/shard_map/reshape | solution.py:47
  232.3 12.2 %fusion.6 = bf16[1,8,128,16,128]{2,4,1,3,0:T(8,128)(2,1)} fusion(f32[1,8,128,16,128]{2,4,1,3,0:T(8,128)} %copy.39, f32[16,8,128,128]{3,2,1,0:T(8,128)} %get-tuple-element.17, f32[8,128,16]{1,0,2:T(8,128)S(1)} %get-tuple-element.18, f32[8,128,16]{1,0,2:T(8,128)S(1)} %get-tuple-element.19, f32[16,128]{1,0:T(8,128)S(1)} %copy-done.3, ...), kind=kLoop, calls=%fused_computation.12 | loop fusion | flops 58720256 | bytes 21241856 | tf_op jit(solution)/shard_map/convert_element_type | solution.py:60
  244.5 6.8 %copy.56 = bf16[1,8,128,16,128]{4,3,2,1,0:T(8,128)(2,1)} copy(bf16[1,8,128,16,128]{2,4,1,3,0:T(8,128)(2,1)} %fusion.6) | data formatting | bytes 8388608 | tf_op jit(solution)/shard_map/convert_element_type | solution.py:60
  251.3 7.3 %reshape.500 = bf16[1,1024,2048]{2,1,0:T(8,128)(2,1)} reshape(bf16[1,8,128,16,128]{4,3,2,1,0:T(8,128)(2,1)} %copy.56) | data formatting | bytes 8388608 | tf_op jit(solution)/shard_map/reshape | solution.py:60
  258.6 112.8 %all-reduce.2.cloned.1.call-done = f32[268288]{0:T(1024)} async-done(((f32[268288]{0:T(1024)}), f32[268288]{0:T(1024)}) %all-reduce.2.cloned.1.call-update) | async-done | bytes 1073168 | tf_op jit(solution)/shard_map/psum | solution.py:22
  371.4 2.3 slice.49
  373.7 1.3 slice_bitcast_fusion
  375.0 194.1 %all-gather.6.cloned.1.call-done = f32[4096,2048]{1,0:T(8,128)} async-done(((f32[256,2048]{1,0:T(8,128)}), f32[4096,2048]{1,0:T(8,128)}) %all-gather.6.cloned.1.call-update) | async-done | bytes 33554448 | tf_op jit(solution)/shard_map/all_gather | solution.py:11
  569.1 13.1 %reduce_sum.76 = f32[256,2048]{1,0:T(8,128)} reduce(f32[16,256,2048]{2,1,0:T(8,128)} %bitcast.107, f32[]{:T(128)} %constant.9.clone.1), dimensions={0}, to_apply=%region_5.6 | reduce | flops 7864320 | bytes 35651588 | tf_op jit(solution)/shard_map/reduce_sum | solution.py:12
  (4 shorter events, 0.1 us)
Async XLA Ops:
  7.2 54.7 %all-gather.4.cloned.1.call-start = ((), (), s32[]{:S(2)}) async-start(), calls=%async_computation.1 | async-start | bytes 9437184 | tf_op jit(solution)/shard_map/all_gather | solution.py:75
  7.9 210.2 %reduce-scatter.2.cloned.1.call-start = ((), (), s32[]{:S(2)}) async-start(), calls=%async_computation.2 | async-start | bytes 18874368 | tf_op jit(solution)/shard_map/reduce_scatter | solution.py:88
  42.7 6.2 %copy-start = (f32[1,8,128,16,128]{2,4,1,3,0:T(8,128)S(1)}, f32[1,8,128,16,128]{2,4,1,3,0:T(8,128)}, u32[]{:S(2)}) copy-start(f32[1,8,128,16,128]{2,4,1,3,0:T(8,128)} %copy.39) | copy-start | bytes 25165828
  42.7 9.9 %copy-start.1 = (f32[128,8,16,128]{3,2,1,0:T(8,128)S(1)}, f32[128,8,16,128]{3,2,1,0:T(8,128)}, u32[]{:S(2)}) copy-start(f32[128,8,16,128]{3,2,1,0:T(8,128)} %copy.65) | copy-start | bytes 25165828
  42.7 9.9 %copy-start.3 = (f32[16,128]{1,0:T(8,128)S(1)}, f32[16,128]{1,0:T(8,128)}, u32[]{:S(2)}) copy-start(f32[16,128]{1,0:T(8,128)} %param.13) | copy-start | bytes 24580
  42.7 9.9 %copy-start.4 = (f32[16,128]{1,0:T(8,128)S(1)}, f32[16,128]{1,0:T(8,128)}, u32[]{:S(2)}) copy-start(f32[16,128]{1,0:T(8,128)} %param.14) | copy-start | bytes 24580
  80.1 8.8 %copy-start.5 = (bf16[16,128,128]{2,1,0:T(8,128)(2,1)S(1)}, bf16[16,128,128]{2,1,0:T(8,128)(2,1)}, u32[]{:S(2)}) copy-start(bf16[16,128,128]{2,1,0:T(8,128)(2,1)} %param.11) | copy-start | bytes 1572868
  80.1 8.8 %copy-start.6 = (f32[16,128]{1,0:T(8,128)S(1)}, f32[16,128]{1,0:T(8,128)}, u32[]{:S(2)}) copy-start(f32[16,128]{1,0:T(8,128)} %param.12) | copy-start | bytes 24580
  126.0 245.4 %all-reduce.2.cloned.1.call-start = ((), (), s32[]{:S(2)}) async-start(), calls=%async_computation.3 | async-start | bytes 2146304 | tf_op jit(solution)/shard_map/psum | solution.py:22
  126.0 10.2 %copy-start.2 = (bf16[8,128,16,128]{3,1,0,2:T(8,128)(2,1)S(1)}, bf16[8,128,16,128]{3,1,0,2:T(8,128)(2,1)}, u32[]{:S(2)}) copy-start(bf16[8,128,16,128]{3,1,0,2:T(8,128)(2,1)} %fusion.35) | copy-start | bytes 12582916
  148.9 420.3 %all-gather.6.cloned.1.call-start = ((), (), s32[]{:S(2)}) async-start(), calls=%async_computation.4 | async-start | bytes 35651584 | tf_op jit(solution)/shard_map/all_gather | solution.py:11
Sparse Core Ops, SparseCore 0:
  9.7 52.0 all-gather.3
  126.1 91.9 reduce-scatter.1
  223.4 147.9 all-reduce.1
  373.4 195.6 all-gather.5
